TPU v7x, 32 devices: a whole 2x2x4 slice. The times are simulated.
32 devices in a mesh: rep: 2 (over x), fs: 4 (over z), tp: 4 (over y, core).
Axes of the slice: x: 2, y: 2, z: 4, core: 2. Of those that a mesh axis runs over, the one named last changes fastest.
Arguments:
- tokens: bfloat16 [4096, 2048], P(('rep', 'fs', 'tp')), may hold values from -6 to 6
- norm1_gain: float32 [2048], replicated, may hold values from 0.1 to 1.9
- in_weight: bfloat16 [2048, 1024], P('fs', 'tp'), may hold values from -0.125 to 0.125
- group_weight: bfloat16 [8, 128, 128], P('tp'), may hold values from -0.5 to 0.5
- pool_scale: float32 [1024], P('tp'), may hold values from 0.1 to 1.9
- out_weight: bfloat16 [1024, 2048], P('tp', 'fs'), may hold values from -0.1875 to 0.1875
- norm2_gain: float32 [2048], replicated, may hold values from 0.1 to 1.9
- up_weight: bfloat16 [2048, 8192], P('fs', 'tp'), may hold values from -0.125 to 0.125
- down_weight: bfloat16 [8192, 2048], P('tp', 'fs'), may hold values from -0.0625 to 0.0625
Outputs:
- layer_out: bfloat16 [4096, 2048], P(('rep', 'fs', 'tp'))
All inputs are finite; a program needn't handle non-finite values.
Results may differ from a plain program's by a relative error of at most 0.02.
Values may be sent and summed in bfloat16 or wider, within the bound.
A program may use at most 128 MiB of HBM per device.

v0:
```python
import jax
import jax.numpy as jnp
from jax import lax
from jax.sharding import PartitionSpec as P

GROUP_DIM = 128
epsilon = 1e-06


def rms_norm(values, gain):
    scale = lax.rsqrt(jnp.mean(values * values, axis=-1, keepdims=True) + epsilon)
    return values * scale * gain


def shifted(values, offset):
    return jnp.pad(values, ((offset, 0), (0, 0)))[: values.shape[0]]


def mix_groups(projected, group_weight, pool_scale):
    length = projected.shape[0]
    local_groups = group_weight.shape[0]
    values = projected.astype(jnp.float32)
    level_sums = []
    running = values
    offset = 1
    for level in range(4):
        running = running + shifted(running, offset)
        offset = offset * 2
        level_sums.append(running)
    first_group = lax.axis_index("tp") * local_groups
    group_level = (first_group + jnp.arange(local_groups, dtype=jnp.int32)) % 4
    column_level = jnp.repeat(group_level, GROUP_DIM)[None, :]
    position = jnp.arange(length, dtype=jnp.int32)[:, None]
    window_mean = jnp.zeros_like(values)
    for level in range(4):
        count = jnp.minimum(position + 1, 2 ** (level + 1)).astype(jnp.float32)
        window_mean = jnp.where(column_level == level, level_sums[level] / count, window_mean)
    pooled = (window_mean - values).astype(jnp.bfloat16).reshape(length, local_groups, GROUP_DIM)
    mapped = jnp.einsum("sgc,gcd->sgd", pooled, group_weight, preferred_element_type=jnp.float32)
    return (mapped.reshape(length, local_groups * GROUP_DIM) * pool_scale).astype(jnp.bfloat16)


def local(
    tokens,
    norm1_gain,
    in_weight,
    group_weight,
    pool_scale,
    out_weight,
    norm2_gain,
    up_weight,
    down_weight,
):
    stream = tokens.astype(jnp.float32)
    normed = rms_norm(stream, norm1_gain).astype(jnp.bfloat16)
    in_local = lax.all_gather(in_weight, "fs", axis=0, tiled=True)
    projected = jnp.dot(
        lax.all_gather(normed, "tp", axis=0, tiled=True),
        in_local,
        preferred_element_type=jnp.float32,
    ).astype(jnp.bfloat16)
    pool_out = mix_groups(projected, group_weight, pool_scale)
    out_local = lax.all_gather(out_weight, "fs", axis=1, tiled=True)
    block_rows = pool_out
    mixed = lax.psum_scatter(
        jnp.dot(block_rows, out_local, preferred_element_type=jnp.float32).astype(jnp.bfloat16),
        "tp",
        scatter_dimension=0,
        tiled=True,
    ).astype(jnp.float32)
    mixed_stream = stream + mixed
    normed_two = rms_norm(mixed_stream, norm2_gain).astype(jnp.bfloat16)
    up_local = lax.all_gather(up_weight, "fs", axis=0, tiled=True)
    upper = jnp.dot(
        lax.all_gather(normed_two, "tp", axis=0, tiled=True),
        up_local,
        preferred_element_type=jnp.float32,
    )
    hidden = jnp.square(jax.nn.relu(upper)).astype(jnp.bfloat16)
    down_local = lax.all_gather(down_weight, "fs", axis=1, tiled=True)
    block_rows = hidden
    channel_sum = lax.psum_scatter(
        jnp.dot(block_rows, down_local, preferred_element_type=jnp.float32).astype(jnp.bfloat16),
        "tp",
        scatter_dimension=0,
        tiled=True,
    ).astype(jnp.float32)
    return (mixed_stream + channel_sum).astype(jnp.bfloat16)


def solution(mesh):
    in_specs = (
        P(("rep", "fs", "tp"), None),
        P(),
        P("fs", "tp"),
        P("tp", None, None),
        P("tp"),
        P("tp", "fs"),
        P(),
        P("fs", "tp"),
        P("tp", "fs"),
    )
    out_specs = P(("rep", "fs", "tp"), None)
    return jax.shard_map(local, mesh=mesh, in_specs=in_specs, out_specs=out_specs, check_vma=False)
```

profile of v0, /device:TPU:0, one launch (start us, length us, event | category | flops | bytes accessed | tf_op | source)
XLA Modules:
  0.0 508.3 jit_solution(7314951836628832567)
XLA Ops:
  6.5 0.7 all-gather.9.cloned.1.call-update
  7.3 1.2 fusion.1
  8.5 2.0 fusion.3
  10.6 0.7 all-gather.11.cloned.1.call-update
  11.5 0.1 broadcast_bitcast_fusion
  11.5 0.1 broadcast_bitcast_fusion.1
  11.7 27.9 %all-gather.9.cloned.1.call-done = bf16[2048,256]{1,0:T(8,128)(2,1)} async-done(((bf16[512,256]{1,0:T(8,128)(2,1)}), bf16[2048,256]{1,0:T(8,128)(2,1)}) %all-gather.9.cloned.1.call-update) | async-done | bytes 1048592 | tf_op jit(solution)/shard_map/all_gather | solution.py:56
  39.6 23.5 %all-gather.7.cloned.1.call-done = bf16[512,2048]{1,0:T(8,128)(2,1)} async-done(((bf16[128,2048]{1,0:T(8,128)(2,1)}), bf16[512,2048]{1,0:T(8,128)(2,1)}) %all-gather.7.cloned.1.call-update) | async-done | bytes 2097168 | tf_op jit(solution)/shard_map/all_gather | solution.py:58
  63.2 2.6 fusion
  66.0 0.7 fusion.13
  66.6 0.1 fusion.11
  66.8 26.0 %all-gather.11.cloned.1.call-done = bf16[256,2048]{1,0:T(8,128)(2,1)} async-done(((bf16[256,512]{1,0:T(8,128)(2,1)}), bf16[256,2048]{1,0:T(8,128)(2,1)}) %all-gather.11.cloned.1.call-update) | async-done | bytes 1048592 | tf_op jit(solution)/shard_map/all_gather | solution.py:63
  92.8 3.3 convolution_convert_fusion
  96.1 30.7 %reduce-scatter.3.cloned.1.call-done = bf16[128,2048]{1,0:T(8,128)(2,1)} async-done(((bf16[512,2048]{1,0:T(8,128)(2,1)}), bf16[128,2048]{1,0:T(8,128)(2,1)}) %reduce-scatter.3.cloned.1.call-update) | async-done | bytes 524304 | tf_op jit(solution)/shard_map/reduce_scatter | solution.py:65
  126.8 1.3 multiply_reduce_fusion
  128.1 2.0 multiply_convert_fusion.1
  130.2 0.5 all-gather.15.cloned.1.call-update
  130.8 0.7 all-gather.17.cloned.1.call-update
  131.6 21.3 %all-gather.13.cloned.1.call-done = bf16[512,2048]{1,0:T(8,128)(2,1)} async-done(((bf16[128,2048]{1,0:T(8,128)(2,1)}), bf16[512,2048]{1,0:T(8,128)(2,1)}) %all-gather.13.cloned.1.call-update) | async-done | bytes 2097168 | tf_op jit(solution)/shard_map/all_gather | solution.py:75
  152.9 151.1 %all-gather.15.cloned.1.call-done = bf16[2048,2048]{1,0:T(8,128)(2,1)} async-done(((bf16[512,2048]{1,0:T(8,128)(2,1)}), bf16[2048,2048]{1,0:T(8,128)(2,1)}) %all-gather.15.cloned.1.call-update) | async-done | bytes 8388624 | tf_op jit(solution)/shard_map/all_gather | solution.py:73
  304.0 149.4 %all-gather.17.cloned.1.call-done = bf16[2048,2048]{1,0:T(8,128)(2,1)} async-done(((bf16[2048,512]{1,0:T(8,128)(2,1)}), bf16[2048,2048]{1,0:T(8,128)(2,1)}) %all-gather.17.cloned.1.call-update) | async-done | bytes 8388624 | tf_op jit(solution)/shard_map/all_gather | solution.py:80
  453.4 16.5 %convolution_convert_fusion.1 = bf16[512,2048]{1,0:T(8,128)(2,1)} fusion(bf16[2048,2048]{1,0:T(8,128)(2,1)} %all-gather.17.cloned.1.call-done, bf16[512,2048]{1,0:T(8,128)(2,1)} %all-gather.13.cloned.1.call-done, bf16[2048,2048]{1,0:T(8,128)(2,1)} %all-gather.15.cloned.1.call-done), kind=kOutput, calls=%fused_computation.2 | convolution fusion | flops 8594128896 | bytes 20971520 | tf_op jit(solution)/shard_map/dot_general | solution.py:83
  469.9 29.5 %reduce-scatter.5.cloned.1.call-done = bf16[128,2048]{1,0:T(8,128)(2,1)} async-done(((bf16[512,2048]{1,0:T(8,128)(2,1)}), bf16[128,2048]{1,0:T(8,128)(2,1)}) %reduce-scatter.5.cloned.1.call-update) | async-done | bytes 524304 | tf_op jit(solution)/shard_map/reduce_scatter | solution.py:82
  499.4 2.1 add_convert_fusion
  (33 shorter events, 0.7 us)
Async XLA Ops:
  6.5 59.4 %copy-start = (bf16[2,128,128]{2,1,0:T(8,128)(2,1)S(1)}, bf16[2,128,128]{2,1,0:T(8,128)(2,1)}, u32[]{:S(2)}) copy-start(bf16[2,128,128]{2,1,0:T(8,128)(2,1)} %param.12) | copy-start | bytes 196612
  6.5 33.1 %all-gather.9.cloned.1.call-start = ((), (), s32[]{:S(2)}) async-start(), calls=%async_computation.3 | async-start | bytes 1310720 | tf_op jit(solution)/shard_map/all_gather | solution.py:56
  7.3 55.9 %all-gather.7.cloned.1.call-start = ((), (), s32[]{:S(2)}) async-start(), calls=%async_computation.2 | async-start | bytes 2621440 | tf_op jit(solution)/shard_map/all_gather | solution.py:58
  10.6 82.2 %all-gather.11.cloned.1.call-start = ((), (), s32[]{:S(2)}) async-start(), calls=%async_computation.4 | async-start | bytes 1310720 | tf_op jit(solution)/shard_map/all_gather | solution.py:63
  11.3 115.5 %reduce-scatter.3.cloned.1.call-start = ((), (), s32[]{:S(2)}) async-start(), calls=%async_computation.5 | async-start | bytes 2621440 | tf_op jit(solution)/shard_map/reduce_scatter | solution.py:65
  65.9 0.7 copy-start.4
  96.1 30.8 %copy-start.1 = (bf16[128,2048]{1,0:T(8,128)(2,1)S(1)}, bf16[128,2048]{1,0:T(8,128)(2,1)}, u32[]{:S(2)}) copy-start(bf16[128,2048]{1,0:T(8,128)(2,1)} %param.9) | copy-start | bytes 1572868
  96.1 32.1 %copy-start.3 = (f32[2048]{0:T(1024)S(1)}, f32[2048]{0:T(1024)}, u32[]{:S(2)}) copy-start(f32[2048]{0:T(1024)} %param.15) | copy-start | bytes 24580
  96.1 56.8 %all-gather.13.cloned.1.call-start = ((), (), s32[]{:S(2)}) async-start(), calls=%async_computation.6 | async-start | bytes 2621440 | tf_op jit(solution)/shard_map/all_gather | solution.py:75
  130.2 173.8 %all-gather.15.cloned.1.call-start = ((), (), s32[]{:S(2)}) async-start(), calls=%async_computation.7 | async-start | bytes 10485760 | tf_op jit(solution)/shard_map/all_gather | solution.py:73
  130.8 322.6 %all-gather.17.cloned.1.call-start = ((), (), s32[]{:S(2)}) async-start(), calls=%async_computation.8 | async-start | bytes 10485760 | tf_op jit(solution)/shard_map/all_gather | solution.py:80
  131.5 367.9 %reduce-scatter.5.cloned.1.call-start = ((), (), s32[]{:S(2)}) async-start(), calls=%async_computation.9 | async-start | bytes 2621440 | tf_op jit(solution)/shard_map/reduce_scatter | solution.py:82
  469.9 29.5 %copy-start.2 = (bf16[128,2048]{1,0:T(8,128)(2,1)S(1)}, bf16[128,2048]{1,0:T(8,128)(2,1)}, u32[]{:S(2)}) copy-start(bf16[128,2048]{1,0:T(8,128)(2,1)} %reduce-scatter.3.cloned.1.call-done) | copy-start | bytes 1572868
Sparse Core Ops, SparseCore 0:
  8.9 30.6 all-gather.8
  41.2 21.9 all-gather.6
  64.7 27.9 all-gather.10
  96.2 30.5 reduce-scatter.2
  130.3 22.5 all-gather.12
  154.3 149.5 all-gather.14
  305.5 147.7 all-gather.16
  470.0 29.3 reduce-scatter.4
where the time goes:
time: 509 us; the launch traced here: 508 us
  waiting for transfers between devices  462 us (91%)
  matrix products  23 us (5%)
  between operations  13.6 us (3%)
  other arithmetic  9 us (2%)
    all_gather x1, waiting for transfers between devices, local(): up_local = lax.all_gather(up_weight, 'fs', axis=0, tiled=True)  151 us
    all_gather x1, waiting for transfers between devices, local(): down_local = lax.all_gather(down_weight, 'fs', axis=1, tiled=True)  149 us
    reduce_scatter x1, waiting for transfers between devices, local(): lax.psum_scatter(jnp.dot(block_rows, out_local, preferred_element_type=jn...  30.7 us
    reduce_scatter x1, waiting for transfers between devices, local(): lax.psum_scatter(jnp.dot(block_rows, down_local, preferred_element_type=j...  29.5 us
    all_gather x1, waiting for transfers between devices, local(): in_local = lax.all_gather(in_weight, 'fs', axis=0, tiled=True)  27.9 us
    all_gather x1, waiting for transfers between devices, local(): out_local = lax.all_gather(out_weight, 'fs', axis=1, tiled=True)  26 us
    all_gather x1, waiting for transfers between devices, local(): lax.all_gather(normed, 'tp', axis=0, tiled=True)  23.5 us
    all_gather x1, waiting for transfers between devices, local(): lax.all_gather(normed_two, 'tp', axis=0, tiled=True)  21.3 us
  transfers between devices with their start and end apart: 8, of which 8 were waited for; matrix products, arithmetic and copies ran while one was open for 1% of the time, Pallas kernels for 0%

commit v1 on v0

--- a/solution.py
+++ b/solution.py
@@ -77,7 +77,12 @@
         preferred_element_type=jnp.float32,
     )
     hidden = jnp.square(jax.nn.relu(upper)).astype(jnp.bfloat16)
-    down_local = lax.all_gather(down_weight, "fs", axis=1, tiled=True)
+    ring = [down_weight]
+    for hop in range(3):
+        ring.append(lax.ppermute(ring[-1], "fs", [(dev, (dev + 1) % 4) for dev in range(4)]))
+    down_local = jnp.roll(
+        jnp.concatenate(ring[::-1], axis=1), (lax.axis_index("fs") + 1) * ring[0].shape[1], axis=1
+    )
     block_rows = hidden
     channel_sum = lax.psum_scatter(
         jnp.dot(block_rows, down_local, preferred_element_type=jnp.float32).astype(jnp.bfloat16),

time: 509 us -> 479 us (0.941)
  waiting for transfers between devices: 462 us -> 346 us
  starting transfers between devices: 0.28 us -> 66.8 us
  local copies, waits for them, and re-layouts: 0.31 us -> 20.2 us
    ppermute x0 -> x3, waiting for transfers between devices: none -> 206 us  [local(): lax.ppermute(ring[-1], 'fs', [(dev, (dev + 1) % 4) for dev in range(4)])]
    all_gather x1, waiting for transfers between devices: 151 us -> 0.01 us  [local(): up_local = lax.all_gather(up_weight, 'fs', axis=0, tiled=True)]
    all_gather x1 -> x0, waiting for transfers between devices: 149 us -> none  [local(): down_local = lax.all_gather(down_weight, 'fs', axis=1, tiled=True)]
    ppermute x0 -> x3, starting transfers between devices: none -> 66.6 us  [local(): lax.ppermute(ring[-1], 'fs', [(dev, (dev + 1) % 4) for dev in range(4)])]
    all_gather x1, waiting for transfers between devices: 21.3 us -> 0.01 us  [local(): lax.all_gather(normed_two, 'tp', axis=0, tiled=True)]
    unnamed x10 -> x23, local copies, waits for them, and re-layouts: 0.02 us -> 18.4 us
  transfers between devices with their start and end apart: 8 -> 10, of which waited for: 8 -> 8; matrix products, arithmetic and copies ran while one was open for 1% -> 5% of each run, Pallas kernels for 0% -> 0%
where the time goes in v1:
time: 479 us; the launch traced here: 478 us
  waiting for transfers between devices  346 us (72%)
  starting transfers between devices  66.8 us (14%)
  matrix products  23.1 us (5%)
  local copies, waits for them, and re-layouts  20.2 us (4%)
  between operations  13.6 us (3%)
  other arithmetic  8.99 us (2%)
    ppermute x3, waiting for transfers between devices, local(): lax.ppermute(ring[-1], 'fs', [(dev, (dev + 1) % 4) for dev in range(4)])  206 us
    ppermute x3, starting transfers between devices, local(): lax.ppermute(ring[-1], 'fs', [(dev, (dev + 1) % 4) for dev in range(4)])  66.6 us
    reduce_scatter x1, waiting for transfers between devices, local(): lax.psum_scatter(jnp.dot(block_rows, out_local, preferred_element_type=jn...  30.7 us
    reduce_scatter x1, waiting for transfers between devices, local(): lax.psum_scatter(jnp.dot(block_rows, down_local, preferred_element_type=j...  29.2 us
    all_gather x1, waiting for transfers between devices, local(): in_local = lax.all_gather(in_weight, 'fs', axis=0, tiled=True)  27.9 us
    all_gather x1, waiting for transfers between devices, local(): out_local = lax.all_gather(out_weight, 'fs', axis=1, tiled=True)  26 us
    all_gather x1, waiting for transfers between devices, local(): lax.all_gather(normed, 'tp', axis=0, tiled=True)  23.5 us
    unnamed x23, local copies, waits for them, and re-layouts  18.4 us
  transfers between devices with their start and end apart: 10, of which 8 were waited for; matrix products, arithmetic and copies ran while one was open for 5% of the time, Pallas kernels for 0%

profile of v1, /device:TPU:0, one launch (start us, length us, event | category | flops | bytes accessed | tf_op | source)
XLA Modules:
  0.0 478.3 jit_solution(14175025263981945486)
XLA Ops:
  8.5 2.0 fusion.8
  11.7 27.9 %all-gather.8.cloned.1.call-done = bf16[2048,256]{1,0:T(8,128)(2,1)} async-done(((bf16[512,256]{1,0:T(8,128)(2,1)}), bf16[2048,256]{1,0:T(8,128)(2,1)}) %all-gather.8.cloned.1.call-update) | async-done | bytes 1048592 | tf_op jit(solution)/shard_map/all_gather | solution.py:56
  39.6 23.5 %all-gather.6.cloned.1.call-done = bf16[512,2048]{1,0:T(8,128)(2,1)} async-done(((bf16[128,2048]{1,0:T(8,128)(2,1)}), bf16[512,2048]{1,0:T(8,128)(2,1)}) %all-gather.6.cloned.1.call-update) | async-done | bytes 2097168 | tf_op jit(solution)/shard_map/all_gather | solution.py:58
  63.2 2.6 fusion.5
  66.8 26.0 %all-gather.10.cloned.1.call-done = bf16[256,2048]{1,0:T(8,128)(2,1)} async-done(((bf16[256,512]{1,0:T(8,128)(2,1)}), bf16[256,2048]{1,0:T(8,128)(2,1)}) %all-gather.10.cloned.1.call-update) | async-done | bytes 1048592 | tf_op jit(solution)/shard_map/all_gather | solution.py:63
  92.8 3.3 convolution_convert_fusion
  96.1 30.7 %reduce-scatter.3.cloned.1.call-done = bf16[128,2048]{1,0:T(8,128)(2,1)} async-done(((bf16[512,2048]{1,0:T(8,128)(2,1)}), bf16[128,2048]{1,0:T(8,128)(2,1)}) %reduce-scatter.3.cloned.1.call-update) | async-done | bytes 524304 | tf_op jit(solution)/shard_map/reduce_scatter | solution.py:65
  128.1 2.0 multiply_convert_fusion.1
  132.3 60.4 %collective-permute-done = bf16[2048,512]{1,0:T(8,128)(2,1)S(1)} collective-permute-done((bf16[2048,512]{1,0:T(8,128)(2,1)S(1)}, bf16[2048,512]{1,0:T(8,128)(2,1)S(1)}, u32[]{:S(2)}, u32[]{:S(2)}) %collective-permute-start) | collective-permute-done | bytes 2097184 | tf_op jit(solution)/shard_map/ppermute | solution.py:82
  194.1 15.6 %collective-permute-start.1 = (bf16[2048,512]{1,0:T(8,128)(2,1)S(1)}, bf16[2048,512]{1,0:T(8,128)(2,1)}, u32[]{:S(2)}, u32[]{:S(2)}) collective-permute-start(bf16[2048,512]{1,0:T(8,128)(2,1)S(1)} %collective-permute-done), channel_id=1, source_target_pairs={{0,4},{4,8},{8,12},{12,0},{1,5},{5,9},{9,13},{13,1},{2,6},{6,10},{... | collective-permute-start | bytes 6291464 | tf_op jit(solution)/shard_map/ppermute | solution.py:82
  209.7 89.2 %collective-permute-done.1 = bf16[2048,512]{1,0:T(8,128)(2,1)} collective-permute-done((bf16[2048,512]{1,0:T(8,128)(2,1)S(1)}, bf16[2048,512]{1,0:T(8,128)(2,1)}, u32[]{:S(2)}, u32[]{:S(2)}) %collective-permute-start.1) | collective-permute-done | bytes 2097184 | tf_op jit(solution)/shard_map/ppermute | solution.py:82
  298.8 49.4 %collective-permute-start.2 = (bf16[2048,512]{1,0:T(8,128)(2,1)}, bf16[2048,512]{1,0:T(8,128)(2,1)}, u32[]{:S(2)}, u32[]{:S(2)}) collective-permute-start(bf16[2048,512]{1,0:T(8,128)(2,1)} %collective-permute-done.1), channel_id=1, source_target_pairs={{0,4},{4,8},{8,12},{12,0},{1,5},{5,9},{9,13},{13,1},{2,6},{6,10},{... | collective-permute-start | bytes 6291464 | tf_op jit(solution)/shard_map/ppermute | solution.py:82
  348.3 56.7 %collective-permute-done.2 = bf16[2048,512]{1,0:T(8,128)(2,1)} collective-permute-done((bf16[2048,512]{1,0:T(8,128)(2,1)}, bf16[2048,512]{1,0:T(8,128)(2,1)}, u32[]{:S(2)}, u32[]{:S(2)}) %collective-permute-start.2) | collective-permute-done | bytes 2097184 | tf_op jit(solution)/shard_map/ppermute | solution.py:82
  405.0 3.1 constant_dynamic-update-slice_fusion.7
  408.1 3.1 constant_dynamic-update-slice_fusion.6
  411.2 1.5 constant_dynamic-update-slice_fusion.5
  412.7 1.5 constant_dynamic-update-slice_fusion.4
  414.3 3.1 constant_dynamic-update-slice_fusion.3
  417.4 3.1 constant_dynamic-update-slice_fusion.2
  420.5 1.5 constant_dynamic-update-slice_fusion.1
  422.0 1.5 constant_dynamic-update-slice_fusion
  423.5 16.6 %fusion.2 = bf16[512,2048]{1,0:T(8,128)(2,1)} fusion(bf16[2048,4096]{1,0:T(8,128)(2,1)} %constant_dynamic-update-slice_fusion, s32[]{:T(128)S(6)} %select_n.38, bf16[512,2048]{1,0:T(8,128)(2,1)} %all-gather.12.cloned.1.call-done, bf16[2048,2048]{1,0:T(8,128)(2,1)} %all-gather.14.cloned.1.call-done), kind=kOutput, calls=%fused_computation.4 | convolution fusion | flops 8594128896 | bytes 20971524 | tf_op jit(solution)/shard_map/dot_general | solution.py:88
  440.2 29.2 %reduce-scatter.5.cloned.1.call-done = bf16[128,2048]{1,0:T(8,128)(2,1)} async-done(((bf16[512,2048]{1,0:T(8,128)(2,1)}), bf16[128,2048]{1,0:T(8,128)(2,1)}) %reduce-scatter.5.cloned.1.call-update) | async-done | bytes 524304 | tf_op jit(solution)/shard_map/reduce_scatter | solution.py:87
  469.4 2.1 add_convert_fusion
  (50 shorter events, 8.9 us)
Async XLA Ops:
  6.5 59.4 %copy-start = (bf16[2,128,128]{2,1,0:T(8,128)(2,1)S(1)}, bf16[2,128,128]{2,1,0:T(8,128)(2,1)}, u32[]{:S(2)}) copy-start(bf16[2,128,128]{2,1,0:T(8,128)(2,1)} %param.12) | copy-start | bytes 196612
  6.5 33.1 %all-gather.8.cloned.1.call-start = ((), (), s32[]{:S(2)}) async-start(), calls=%async_computation.3 | async-start | bytes 1310720 | tf_op jit(solution)/shard_map/all_gather | solution.py:56
  7.3 55.9 %all-gather.6.cloned.1.call-start = ((), (), s32[]{:S(2)}) async-start(), calls=%async_computation.2 | async-start | bytes 2621440 | tf_op jit(solution)/shard_map/all_gather | solution.py:58
  10.6 82.2 %all-gather.10.cloned.1.call-start = ((), (), s32[]{:S(2)}) async-start(), calls=%async_computation.4 | async-start | bytes 1310720 | tf_op jit(solution)/shard_map/all_gather | solution.py:63
  11.3 115.5 %reduce-scatter.3.cloned.1.call-start = ((), (), s32[]{:S(2)}) async-start(), calls=%async_computation.5 | async-start | bytes 2621440 | tf_op jit(solution)/shard_map/reduce_scatter | solution.py:65
  65.9 0.7 copy-start.7
  66.6 60.2 %copy-start.1 = (bf16[128,2048]{1,0:T(8,128)(2,1)S(1)}, bf16[128,2048]{1,0:T(8,128)(2,1)}, u32[]{:S(2)}) copy-start(bf16[128,2048]{1,0:T(8,128)(2,1)} %param.9) | copy-start | bytes 1572868
  66.7 61.5 %copy-start.6 = (f32[2048]{0:T(1024)S(1)}, f32[2048]{0:T(1024)}, u32[]{:S(2)}) copy-start(f32[2048]{0:T(1024)} %param.15) | copy-start | bytes 24580
  96.1 34.8 %copy-start.2 = (bf16[2048,512]{1,0:T(8,128)(2,1)S(1)}, bf16[2048,512]{1,0:T(8,128)(2,1)}, u32[]{:S(2)}) copy-start(bf16[2048,512]{1,0:T(8,128)(2,1)} %param.17) | copy-start | bytes 6291460
  96.1 327.5 %all-gather.12.cloned.1.call-start = ((), (), s32[]{:S(2)}) async-start(), calls=%async_computation.6 | async-start | bytes 2621440 | tf_op jit(solution)/shard_map/all_gather | solution.py:75
  130.2 293.4 %all-gather.14.cloned.1.call-start = ((), (), s32[]{:S(2)}) async-start(), calls=%async_computation.7 | async-start | bytes 10485760 | tf_op jit(solution)/shard_map/all_gather | solution.py:73
  130.8 338.6 %reduce-scatter.5.cloned.1.call-start = ((), (), s32[]{:S(2)}) async-start(), calls=%async_computation.8 | async-start | bytes 2621440 | tf_op jit(solution)/shard_map/reduce_scatter | solution.py:87
  130.8 61.9 %collective-permute-start = (bf16[2048,512]{1,0:T(8,128)(2,1)S(1)}, bf16[2048,512]{1,0:T(8,128)(2,1)S(1)}, u32[]{:S(2)}, u32[]{:S(2)}) collective-permute-start(bf16[2048,512]{1,0:T(8,128)(2,1)S(1)} %copy-done.2), channel_id=1, source_target_pairs={{0,4},{4,8},{8,12},{12,0},{1,5},{5,9},{9,13},{13,1},{2,6},{6,10},{... | collective-permute-start | bytes 6291464 | tf_op jit(solution)/shard_map/ppermute | solution.py:82
  192.8 1.3 copy-start.3
  194.1 104.8 %collective-permute-start.1 = (bf16[2048,512]{1,0:T(8,128)(2,1)S(1)}, bf16[2048,512]{1,0:T(8,128)(2,1)}, u32[]{:S(2)}, u32[]{:S(2)}) collective-permute-start(bf16[2048,512]{1,0:T(8,128)(2,1)S(1)} %collective-permute-done), channel_id=1, source_target_pairs={{0,4},{4,8},{8,12},{12,0},{1,5},{5,9},{9,13},{13,1},{2,6},{6,10},{... | collective-permute-start | bytes 6291464 | tf_op jit(solution)/shard_map/ppermute | solution.py:82
  298.8 106.2 %collective-permute-start.2 = (bf16[2048,512]{1,0:T(8,128)(2,1)}, bf16[2048,512]{1,0:T(8,128)(2,1)}, u32[]{:S(2)}, u32[]{:S(2)}) collective-permute-start(bf16[2048,512]{1,0:T(8,128)(2,1)} %collective-permute-done.1), channel_id=1, source_target_pairs={{0,4},{4,8},{8,12},{12,0},{1,5},{5,9},{9,13},{13,1},{2,6},{6,10},{... | collective-permute-start | bytes 6291464 | tf_op jit(solution)/shard_map/ppermute | solution.py:82
  348.3 62.9 %copy-start.4 = (bf16[2048,512]{1,0:T(8,128)(2,1)S(1)}, bf16[2048,512]{1,0:T(8,128)(2,1)}, u32[]{:S(2)}) copy-start(bf16[2048,512]{1,0:T(8,128)(2,1)} %copy-done.3) | copy-start | bytes 6291460
  423.5 45.9 %copy-start.5 = (bf16[128,2048]{1,0:T(8,128)(2,1)S(1)}, bf16[128,2048]{1,0:T(8,128)(2,1)}, u32[]{:S(2)}) copy-start(bf16[128,2048]{1,0:T(8,128)(2,1)} %reduce-scatter.3.cloned.1.call-done) | copy-start | bytes 1572868
Sparse Core Ops, SparseCore 0:
  8.9 30.6 all-gather.7
  41.2 21.9 all-gather.5
  64.7 27.9 all-gather.9
  96.2 30.5 reduce-scatter.2
  130.3 22.5 all-gather.11
  154.3 220.4 all-gather.13
  440.3 29.0 reduce-scatter.4
